TPU v7x, 256 devices: a whole 4x4x8 slice. The times are simulated.
256 devices in a mesh: ep: 64 (over z, y, core), tp: 4 (over x).
Axes of the slice: x: 4, y: 4, z: 8, core: 2. Of those that a mesh axis runs over, the one named last changes fastest.
Arguments:
- tokens: bfloat16 [1024, 2048], P('ep'), may hold values from -6 to 6
- norm_gain: float32 [2048], replicated, may hold values from 0.1 to 1.9
- query_weight: bfloat16 [2048, 1024], P(None, 'tp'), may hold values from -0.21875 to 0.21875
- key_weight: bfloat16 [2048, 512], P(None, 'tp'), may hold values from -0.125 to 0.125
- value_weight: bfloat16 [2048, 512], P(None, 'tp'), may hold values from -0.125 to 0.125
- output_weight: bfloat16 [1024, 2048], P('tp'), may hold values from -0.1875 to 0.1875
- head_gain: float32 [128], replicated, may hold values from 0.1 to 1.9
- lambdas: float32 [8], P('tp'), may hold values from 0.3 to 0.8
- key_cache: bfloat16 [1024, 1024, 4, 128], P('ep', None, 'tp')
- value_cache: bfloat16 [1024, 1024, 4, 128], P('ep', None, 'tp'), may hold values from -6 to 6
- lengths: int32 [1024], P('ep'), may hold values from 128 to 1024, as said below
- ffn_gain: float32 [2048], replicated, may hold values from 0.1 to 1.9
- routes: int32 [1024, 4], P('ep'), may hold values from 0 to 63, all different within a row; in each aligned block of 16 rows (0 to 15, 16 to 31, ...) at most 2 rows name the same one
- route_weight: float32 [1024, 4], P('ep'), may hold values from 0.1 to 1
- expert_gate: bfloat16 [64, 2048, 1024], P('ep', None, 'tp'), may hold values from -0.125 to 0.125
- expert_up: bfloat16 [64, 2048, 1024], P('ep', None, 'tp'), may hold values from -0.125 to 0.125
- expert_down: bfloat16 [64, 1024, 2048], P('ep', 'tp'), may hold values from -0.1875 to 0.1875
- dense_gate: bfloat16 [2048, 2048], P('tp'), may hold values from -0.125 to 0.125
- dense_up: bfloat16 [2048, 2048], P('tp'), may hold values from -0.125 to 0.125
- dense_down: bfloat16 [2048, 2048], P('tp'), may hold values from -0.1875 to 0.1875
- gate_vector: float32 [2048], P('tp')
Outputs:
- layer_out: bfloat16 [1024, 2048], P('ep', 'tp')
Inputs may be any that keep to these rules, and one draw needn't show every extreme that they name: `routes`: each row names 4 different experts. Among the rows of one index of ep no expert is named by more than 2 rows, a bound that some block reaches. `lengths`: some sequence has length 1024. Cached positions at or past a sequence's length are not read.
All inputs are finite; a program needn't handle non-finite values.
Results may differ from a plain program's by a relative error of at most 0.015.
The roundings to bfloat16 on the way count: a program that leaves them out, or rounds other values in their place, can miss the bound.
Values may be sent and summed in bfloat16 or wider, within the bound.
A program may use at most 128 MiB of HBM per device.

v0:
```python
import jax
import jax.numpy as jnp
from jax import lax
from jax.sharding import PartitionSpec as P

HEADS = 8
KV_HEADS = 4
DQK = 64
DV = 128
TOPK = 4


epsilon = 1e-06


def from_everyone(shard, axis):
    devices = lax.axis_size(axis)
    return lax.all_to_all(
        jnp.broadcast_to(shard[None], (devices, *shard.shape)), axis, 0, 0, tiled=True
    )


def taken_together(shard, axis):
    return from_everyone(shard, axis).astype(jnp.float32).sum(axis=0)


def of_everyone(shard, axis):
    everything = from_everyone(shard, axis)
    return jnp.sum(everything, axis=0)


def cut_along(shard, dim, devices):
    before, after = (shard.shape[:dim], shard.shape[dim + 1 :])
    return jnp.moveaxis(shard.reshape(*before, devices, -1, *after), dim, 0)


def sent_and_summed(shard, axis, dim):
    devices = lax.axis_size(axis)
    blocks = lax.all_to_all(cut_along(shard, dim, devices), axis, 0, 0, tiled=True)
    return jnp.sum(blocks.astype(jnp.float32), axis=0)


def rms_scale(values, gain):
    return values * lax.rsqrt(jnp.mean(values * values, axis=-1, keepdims=True) + epsilon) * gain


def expert_hidden_rows(flat_rows, expert_gate, expert_up):
    expert_pre = jnp.dot(flat_rows, expert_gate[0], preferred_element_type=jnp.float32)
    expert_upper = jnp.dot(flat_rows, expert_up[0], preferred_element_type=jnp.float32)
    return (jax.nn.silu(expert_pre) * expert_upper).astype(jnp.bfloat16)


def shards(
    tokens,
    norm_gain,
    query_weight,
    key_weight,
    value_weight,
    output_weight,
    head_gain,
    lambdas,
    key_cache,
    value_cache,
    lengths,
    ffn_gain,
    routes,
    route_weight,
    expert_gate,
    expert_up,
    expert_down,
    dense_gate,
    dense_up,
    dense_down,
    gate_vector,
):
    seq_count = tokens.shape[0]
    model_width = tokens.shape[1]
    cache_len = key_cache.shape[1]
    local_kv = key_cache.shape[2]
    group_size = HEADS // KV_HEADS
    tokens_wide = tokens.astype(jnp.float32)
    normed = rms_scale(tokens_wide, norm_gain).astype(jnp.bfloat16)
    queries = jnp.dot(normed, query_weight, preferred_element_type=jnp.float32).astype(jnp.bfloat16)
    queries = queries.reshape(seq_count, local_kv, group_size, 2, DQK)
    new_keys = jnp.dot(normed, key_weight, preferred_element_type=jnp.float32).astype(jnp.bfloat16)
    new_keys = new_keys.reshape(seq_count, local_kv, 2, DQK)
    new_values = jnp.dot(normed, value_weight, preferred_element_type=jnp.float32).astype(
        jnp.bfloat16
    )
    new_values = new_values.reshape(seq_count, local_kv, DV)
    key_rows = key_cache.reshape(seq_count, cache_len, local_kv, 2, DQK)
    score_scale = DQK ** (-0.5)
    cache_scores = (
        jnp.einsum("skgmd,sckmd->skgmc", queries, key_rows, preferred_element_type=jnp.float32)
        * score_scale
    )
    own_score = (
        jnp.einsum("skgmd,skmd->skgm", queries, new_keys, preferred_element_type=jnp.float32)
        * score_scale
    )
    live_mask = jnp.arange(cache_len)[None, :] < lengths[:, None]
    cache_scores = jnp.where(live_mask[:, None, None, None, :], cache_scores, -jnp.inf)
    top_score = jnp.maximum(jnp.max(cache_scores, axis=-1), own_score)
    cache_exp = jnp.exp(cache_scores - top_score[..., None])
    own_exp = jnp.exp(own_score - top_score)
    totals = jnp.sum(cache_exp, axis=-1) + own_exp
    cache_prob = cache_exp / totals[..., None]
    own_prob = own_exp / totals
    lambda_grid = lambdas.reshape(local_kv, group_size)
    cache_weight = (
        cache_prob[:, :, :, 0] - lambda_grid[None, :, :, None] * cache_prob[:, :, :, 1]
    ).astype(jnp.bfloat16)
    own_weight = (own_prob[..., 0] - lambda_grid[None] * own_prob[..., 1]).astype(jnp.bfloat16)
    mixture = jnp.einsum(
        "skgc,sckv->skgv", cache_weight, value_cache, preferred_element_type=jnp.float32
    )
    mixture = (
        mixture
        + own_weight.astype(jnp.float32)[..., None] * new_values.astype(jnp.float32)[:, :, None, :]
    )
    head_rows = rms_scale(mixture, head_gain).astype(jnp.bfloat16).reshape(seq_count, -1)
    partial_value = jnp.dot(head_rows, output_weight, preferred_element_type=jnp.float32)
    attention = taken_together(partial_value.astype(jnp.bfloat16), "tp").astype(jnp.float32)
    residual = tokens_wide + attention
    ffn_in = rms_scale(residual, ffn_gain).astype(jnp.bfloat16)
    contract = (((1,), (1,)), ((), ()))
    gate_pre = lax.dot_general(ffn_in, dense_gate, contract, preferred_element_type=jnp.float32)
    up_proj = lax.dot_general(ffn_in, dense_up, contract, preferred_element_type=jnp.float32)
    dense_hidden = (jax.nn.silu(gate_pre) * up_proj).astype(jnp.bfloat16)
    logit_part = jnp.sum(dense_hidden.astype(jnp.float32) * gate_vector, axis=-1)
    dense_term = jnp.dot(dense_hidden, dense_down, preferred_element_type=jnp.float32)
    gate_logit = of_everyone(logit_part, "tp")
    dense_sum = sent_and_summed(dense_term.astype(jnp.bfloat16), "tp", 1)
    dense_out = jax.nn.sigmoid(gate_logit)[:, None] * dense_sum
    experts_total = lax.axis_size("ep")
    capacity = max(2, 2 * seq_count * TOPK // experts_total)
    slot_total = experts_total * capacity
    pair_expert = routes.reshape(-1)
    onehot = (pair_expert[:, None] == jnp.arange(experts_total, dtype=jnp.int32)[None, :]).astype(
        jnp.int32
    )
    slot_rank = jnp.sum(jnp.cumsum(onehot, axis=0) * onehot, axis=1) - 1
    slot_index = pair_expert * capacity + slot_rank
    dispatch = jnp.sum(
        slot_index.reshape(seq_count, TOPK)[None, :, :]
        == jnp.arange(slot_total, dtype=jnp.int32)[:, None, None],
        axis=2,
    )
    outbound = jnp.dot(dispatch.astype(jnp.bfloat16), ffn_in, preferred_element_type=jnp.float32)
    outbound = outbound.astype(jnp.bfloat16).reshape(experts_total, capacity, model_width)
    arrived = lax.all_to_all(outbound, "ep", split_axis=0, concat_axis=0, tiled=True)
    sources, items, width = arrived.shape
    hidden_rows = expert_hidden_rows(arrived.reshape(-1, width), expert_gate, expert_up)
    expert_part = jnp.dot(hidden_rows, expert_down[0], preferred_element_type=jnp.float32)
    expert_part = expert_part.reshape(sources, items, width)
    summed = sent_and_summed(expert_part.astype(jnp.bfloat16), "tp", 2).astype(jnp.bfloat16)
    returned = lax.all_to_all(summed, "ep", split_axis=0, concat_axis=0, tiled=True)
    flat_back = returned.reshape(slot_total, -1)
    picked = flat_back[slot_index].reshape(seq_count, TOPK, -1).astype(jnp.float32)
    expert_mix = jnp.sum(picked * route_weight[:, :, None], axis=1)
    own_columns = model_width // lax.axis_size("tp")
    residual_part = lax.dynamic_slice_in_dim(
        residual, lax.axis_index("tp") * own_columns, own_columns, 1
    )
    return (residual_part + expert_mix + dense_out).astype(jnp.bfloat16)


def solution(mesh):
    placed = (
        P("ep", None),
        P(),
        P(None, "tp"),
        P(None, "tp"),
        P(None, "tp"),
        P("tp", None),
        P(),
        P("tp"),
        P("ep", None, "tp", None),
        P("ep", None, "tp", None),
        P("ep"),
        P(),
        P("ep", None),
        P("ep", None),
        P("ep", None, "tp"),
        P("ep", None, "tp"),
        P("ep", "tp", None),
        P("tp", None),
        P("tp", None),
        P("tp", None),
        P("tp"),
    )
    return jax.shard_map(
        shards, mesh=mesh, in_specs=placed, out_specs=P("ep", "tp"), check_vma=False
    )
```

profile of v0, /device:TPU:1, one launch (start us, length us, event | category | flops | bytes accessed | tf_op | source)
XLA Modules:
  0.0 114.0 jit_solution(5457715531044594561)
XLA Ops:
  0.0 1.1 fusion.17
  1.1 1.6 %convolution_convert_fusion.4 = bf16[16,256]{1,0:T(8,128)(2,1)S(1)} fusion(bf16[2048,256]{1,0:T(8,128)(2,1)} %param.23, bf16[16,2048]{1,0:T(8,128)(2,1)} %param.21, f32[2048]{0:T(1024)} %param.22, f32[16]{0:T(128)S(1)} %add_rsqrt_fusion.2), kind=kOutput, calls=%fused_computation.16 | convolution fusion | flops 16912384 | bytes 1130560 | tf_op jit(solution)/shard_map/dot_general | solution.py:83
  2.8 1.3 %convolution_convert_fusion.6 = bf16[16,128]{1,0:T(8,128)(2,1)S(1)} fusion(bf16[2048,128]{1,0:T(8,128)(2,1)} %param.24, bf16[16,2048]{1,0:T(8,128)(2,1)} %param.21, f32[2048]{0:T(1024)} %param.22, f32[16]{0:T(128)S(1)} %add_rsqrt_fusion.2), kind=kOutput, calls=%fused_computation.19 | convolution fusion | flops 8521728 | bytes 602176 | tf_op jit(solution)/shard_map/dot_general | solution.py:85
  4.5 6.4 %copy.96 = bf16[16,1024,1,128]{1,3,0,2:T(8,128)(2,1)} copy(bf16[16,1024,1,128]{3,1,2,0:T(8,128)(2,1)} %param.29) | data formatting | bytes 8388608 | tf_op args[8]
  11.0 3.0 %fusion.43 = (f32[16,2,2]{1,2,0:T(2,128)S(1)}, f32[16,1,2,2,1024]{4,2,3,0,1:T(2,128)S(1)}) fusion(bf16[16,1024,2,64]{1,3,2,0:T(8,128)(2,1)} %bitcast.128, bf16[16,2,2,64]{3,2,1,0:T(2,128)(2,1)S(1)} %reshape.216, pred[16,1024]{1,0:T(8,128)(4,1)S(1)} %iota_compare_fusion), kind=kOutput, calls=%fused_computation.85 | convolution fusion | flops 8585152 | bytes 4481280 | tf_op jit(solution)/shard_map/skgmd,sckmd->skgmc/dot_general | solution.py:94
  14.2 0.3 fusion.16
  15.5 3.1 %multiply_reduce_fusion.3 = (f32[16,2]{1,0:T(8,128)S(1)}, f32[16,2,128]{2,1,0:T(2,128)S(1)}) fusion(f32[16,128]{1,0:T(8,128)S(1)} %fusion.10, f32[16,2]{1,0:T(8,128)S(1)} %copy.104, bf16[16,1024,1,128]{3,1,2,0:T(8,128)(2,1)} %param.30, f32[16,1,2,2,1024]{4,2,3,0,1:T(2,128)S(1)} %fusion.15, f32[2]{0:T(128)S(1)} %copy-done.7), kind=kOutput, calls=%fused_computation.55 | convolution fusion | flops 8503264 | bytes 4481288 | tf_op jit(solution)/shard_map/skgc,sckv->skgv/dot_general | solution.py:114
  19.0 0.7 broadcast_in_dim.18
  19.7 4.8 %all-to-all-start = ((bf16[4,16,2048]{2,1,0:T(8,128)(2,1)}), bf16[4,16,2048]{2,1,0:T(8,128)(2,1)S(1)}, u32[]{:S(2)}, u32[]{:S(2)}) async-start(bf16[4,16,2048]{2,1,0:T(8,128)(2,1)} %broadcast_in_dim.18), calls=%async_computation | async-start | bytes 524288 | tf_op jit(solution)/shard_map/all_to_all | solution.py:18
  25.3 4.7 %all-to-all-done = bf16[4,16,2048]{2,1,0:T(8,128)(2,1)S(1)} async-done(((bf16[4,16,2048]{2,1,0:T(8,128)(2,1)}), bf16[4,16,2048]{2,1,0:T(8,128)(2,1)S(1)}, u32[]{:S(2)}, u32[]{:S(2)}) %all-to-all-start) | async-done | bytes 262176 | tf_op jit(solution)/shard_map/all_to_all | solution.py:18
  30.7 1.1 reshape.221
  31.8 13.8 %all-to-all-start.1 = ((bf16[64,2,2048]{2,1,0:T(2,128)(2,1)}), bf16[64,2,2048]{2,1,0:T(2,128)(2,1)S(1)}, u32[]{:S(2)}, u32[]{:S(2)}) async-start(bf16[64,2,2048]{2,1,0:T(2,128)(2,1)} %reshape.221), calls=%async_computation.1 | async-start | bytes 1048576 | tf_op jit(solution)/shard_map/all_to_all | solution.py:151
  45.6 2.4 %fusion.44 = f32[16,512]{1,0:T(8,128)S(1)} fusion(bf16[16,2048]{1,0:T(8,128)(2,1)S(1)} %multiply_convert_fusion, bf16[512,2048]{1,0:T(8,128)(2,1)} %param.38), kind=kOutput, calls=%fused_computation.86 | convolution fusion | flops 33554432 | bytes 2195456 | tf_op jit(solution)/shard_map/dot_general | solution.py:127
  48.0 0.8 multiply_reduce_fusion.2
  48.8 14.4 %all-to-all-done.1 = bf16[64,2,2048]{2,1,0:T(2,128)(2,1)S(1)} async-done(((bf16[64,2,2048]{2,1,0:T(2,128)(2,1)}), bf16[64,2,2048]{2,1,0:T(2,128)(2,1)S(1)}, u32[]{:S(2)}, u32[]{:S(2)}) %all-to-all-start.1) | async-done | bytes 524320 | tf_op jit(solution)/shard_map/all_to_all | solution.py:151
  63.2 0.6 broadcast_in_dim.19
  63.8 3.2 %all-to-all-start.4 = ((f32[4,1,16]{2,1,0:T(1,128)}), f32[4,1,16]{2,1,0:T(1,128)S(1)}, u32[]{:S(2)}, u32[]{:S(2)}) async-start(f32[4,1,16]{2,1,0:T(1,128)} %broadcast_in_dim.19), calls=%async_computation.4 | async-start | bytes 4096 | tf_op jit(solution)/shard_map/all_to_all | solution.py:18
  67.3 1.5 %fusion.13 = f32[128,256]{1,0:T(8,128)S(1)} fusion(bf16[128,2048]{1,0:T(8,128)(2,1)S(1)} %reshape.222, bf16[1,2048,256]{2,1,0:T(8,128)(2,1)} %param.35), kind=kOutput, calls=%fused_computation.22 | convolution fusion | flops 134217728 | bytes 1703936 | tf_op jit(solution)/shard_map/dot_general | solution.py:48
  68.8 1.5 %fusion.5 = bf16[128,256]{1,0:T(8,128)(2,1)S(1)} fusion(bf16[128,2048]{1,0:T(8,128)(2,1)S(1)} %reshape.222, bf16[1,2048,256]{2,1,0:T(8,128)(2,1)} %param.36, f32[128,256]{1,0:T(8,128)S(1)} %fusion.13), kind=kOutput, calls=%fused_computation.12 | convolution fusion | flops 134414336 | bytes 1769472 | tf_op jit(solution)/shard_map/dot_general | solution.py:49
  70.4 1.5 %convolution_convert_fusion = bf16[64,2,2048]{2,0,1:T(8,128)(2,1)S(1)} fusion(bf16[1,256,2048]{2,1,0:T(8,128)(2,1)} %param.37, bf16[64,2,256]{2,1,0:T(2,128)(2,1)S(1)} %dot_general.54), kind=kOutput, calls=%fused_computation.3 | convolution fusion | flops 134479872 | bytes 1638400 | tf_op jit(solution)/shard_map/dot_general | solution.py:154
  71.9 0.8 copy.142
  72.8 4.2 %all-to-all-start.2 = ((bf16[4,64,2,512]{3,1,2,0:T(8,128)(2,1)}), bf16[4,64,2,512]{3,1,2,0:T(8,128)(2,1)S(1)}, u32[]{:S(2)}, u32[]{:S(2)}) async-start(bf16[4,64,2,512]{3,1,2,0:T(8,128)(2,1)} %bitcast.125), calls=%async_computation.2 | async-start | bytes 1048576 | tf_op jit(solution)/shard_map/all_to_all | solution.py:39
  77.0 0.4 convolution_convert_fusion.2
  77.4 0.6 copy.143
  78.0 7.3 %all-to-all-done.2 = bf16[4,64,2,512]{3,1,2,0:T(8,128)(2,1)S(1)} async-done(((bf16[4,64,2,512]{3,1,2,0:T(8,128)(2,1)}), bf16[4,64,2,512]{3,1,2,0:T(8,128)(2,1)S(1)}, u32[]{:S(2)}, u32[]{:S(2)}) %all-to-all-start.2) | async-done | bytes 524320 | tf_op jit(solution)/shard_map/all_to_all | solution.py:39
  85.3 3.3 %all-to-all-start.5 = ((bf16[4,16,512]{2,1,0:T(8,128)(2,1)}), bf16[4,16,512]{2,1,0:T(8,128)(2,1)S(1)}, u32[]{:S(2)}, u32[]{:S(2)}) async-start(bf16[4,16,512]{2,1,0:T(8,128)(2,1)} %bitcast.127), calls=%async_computation.5 | async-start | bytes 131072 | tf_op jit(solution)/shard_map/all_to_all | solution.py:39
  88.8 0.8 copy.111
  89.6 3.5 %all-to-all-done.5 = bf16[4,16,512]{2,1,0:T(8,128)(2,1)S(1)} async-done(((bf16[4,16,512]{2,1,0:T(8,128)(2,1)}), bf16[4,16,512]{2,1,0:T(8,128)(2,1)S(1)}, u32[]{:S(2)}, u32[]{:S(2)}) %all-to-all-start.5) | async-done | bytes 65568 | tf_op jit(solution)/shard_map/all_to_all | solution.py:39
  93.0 8.2 %all-to-all-start.3 = ((bf16[64,2,512]{2,1,0:T(2,128)(2,1)}), bf16[64,2,512]{2,1,0:T(2,128)(2,1)S(1)}, u32[]{:S(2)}, u32[]{:S(2)}) async-start(bf16[64,2,512]{2,1,0:T(2,128)(2,1)} %copy.111), calls=%async_computation.3 | async-start | bytes 262144 | tf_op jit(solution)/shard_map/all_to_all | solution.py:157
  101.3 11.1 %all-to-all-done.3 = bf16[64,2,512]{2,1,0:T(2,128)(2,1)S(1)} async-done(((bf16[64,2,512]{2,1,0:T(2,128)(2,1)}), bf16[64,2,512]{2,1,0:T(2,128)(2,1)S(1)}, u32[]{:S(2)}, u32[]{:S(2)}) %all-to-all-start.3) | async-done | bytes 131104 | tf_op jit(solution)/shard_map/all_to_all | solution.py:157
  112.4 0.7 gather_fusion
  113.3 0.7 add_convert_fusion
  (75 shorter events, 4.2 us)
Async XLA Ops:
  0.0 77.0 %copy-start = (bf16[512,2048]{1,0:T(8,128)(2,1)S(1)}, bf16[512,2048]{1,0:T(8,128)(2,1)}, u32[]{:S(2)}) copy-start(bf16[512,2048]{1,0:T(8,128)(2,1)} %param.40) | copy-start | bytes 6291460
  4.5 6.4 %copy-start.12 = (s32[16]{0:T(128)S(1)}, s32[16]{0:T(128)}, u32[]{:S(2)}) copy-start(s32[16]{0:T(128)} %param.31) | copy-start | bytes 196
  11.0 4.1 %copy-start.7 = (f32[2]{0:T(128)S(1)}, f32[2]{0:T(128)}, u32[]{:S(2)}) copy-start(f32[2]{0:T(128)} %param.28) | copy-start | bytes 28
  11.0 4.3 %copy-start.2 = (bf16[16,2048]{1,0:T(8,128)(2,1)S(1)}, bf16[16,2048]{1,0:T(8,128)(2,1)}, u32[]{:S(2)}) copy-start(bf16[16,2048]{1,0:T(8,128)(2,1)} %param.21) | copy-start | bytes 196612
  11.0 4.3 %copy-start.4 = (bf16[2048,128]{1,0:T(8,128)(2,1)S(1)}, bf16[2048,128]{1,0:T(8,128)(2,1)}, u32[]{:S(2)}) copy-start(bf16[2048,128]{1,0:T(8,128)(2,1)} %param.25) | copy-start | bytes 1572868
  11.0 4.2 %copy-start.5 = (f32[2048]{0:T(1024)S(1)}, f32[2048]{0:T(1024)}, u32[]{:S(2)}) copy-start(f32[2048]{0:T(1024)} %param.22) | copy-start | bytes 24580
  15.5 3.1 %copy-start.11 = (f32[128]{0:T(128)S(1)}, f32[128]{0:T(128)}, u32[]{:S(2)}) copy-start(f32[128]{0:T(128)} %param.27) | copy-start | bytes 1540
  15.5 3.2 %copy-start.3 = (bf16[256,2048]{1,0:T(8,128)(2,1)S(1)}, bf16[256,2048]{1,0:T(8,128)(2,1)}, u32[]{:S(2)}) copy-start(bf16[256,2048]{1,0:T(8,128)(2,1)} %param.26) | copy-start | bytes 3145732
  15.5 9.0 %copy-start.8 = (s32[16,4]{0,1:T(4,128)S(1)}, s32[16,4]{0,1:T(4,128)}, u32[]{:S(2)}) copy-start(s32[16,4]{0,1:T(4,128)} %param.33) | copy-start | bytes 772
  18.6 11.6 %copy-start.6 = (f32[2048]{0:T(1024)S(1)}, f32[2048]{0:T(1024)}, u32[]{:S(2)}) copy-start(f32[2048]{0:T(1024)} %param.32) | copy-start | bytes 24580
  19.7 10.4 %all-to-all-start = ((bf16[4,16,2048]{2,1,0:T(8,128)(2,1)}), bf16[4,16,2048]{2,1,0:T(8,128)(2,1)S(1)}, u32[]{:S(2)}, u32[]{:S(2)}) async-start(bf16[4,16,2048]{2,1,0:T(8,128)(2,1)} %broadcast_in_dim.18), calls=%async_computation | async-start | bytes 524288 | tf_op jit(solution)/shard_map/all_to_all | solution.py:18
  30.6 17.4 %copy-start.10 = (f32[512]{0:T(512)S(1)}, f32[512]{0:T(512)}, u32[]{:S(2)}) copy-start(f32[512]{0:T(512)} %param.41) | copy-start | bytes 6148
  31.8 31.5 %all-to-all-start.1 = ((bf16[64,2,2048]{2,1,0:T(2,128)(2,1)}), bf16[64,2,2048]{2,1,0:T(2,128)(2,1)S(1)}, u32[]{:S(2)}, u32[]{:S(2)}) async-start(bf16[64,2,2048]{2,1,0:T(2,128)(2,1)} %reshape.221), calls=%async_computation.1 | async-start | bytes 1048576 | tf_op jit(solution)/shard_map/all_to_all | solution.py:151
  45.6 2.4 %copy-start.1 = (bf16[512,2048]{1,0:T(8,128)(2,1)S(1)}, bf16[512,2048]{1,0:T(8,128)(2,1)}, u32[]{:S(2)}) copy-start(bf16[512,2048]{1,0:T(8,128)(2,1)} %param.39) | copy-start | bytes 6291460
  63.8 9.0 %all-to-all-start.4 = ((f32[4,1,16]{2,1,0:T(1,128)}), f32[4,1,16]{2,1,0:T(1,128)S(1)}, u32[]{:S(2)}, u32[]{:S(2)}) async-start(f32[4,1,16]{2,1,0:T(1,128)} %broadcast_in_dim.19), calls=%async_computation.4 | async-start | bytes 4096 | tf_op jit(solution)/shard_map/all_to_all | solution.py:18
  71.9 16.7 %copy-start.9 = (f32[16,4]{0,1:T(4,128)S(1)}, f32[16,4]{0,1:T(4,128)}, u32[]{:S(2)}) copy-start(f32[16,4]{0,1:T(4,128)} %param.34) | copy-start | bytes 772
  72.8 12.5 %all-to-all-start.2 = ((bf16[4,64,2,512]{3,1,2,0:T(8,128)(2,1)}), bf16[4,64,2,512]{3,1,2,0:T(8,128)(2,1)S(1)}, u32[]{:S(2)}, u32[]{:S(2)}) async-start(bf16[4,64,2,512]{3,1,2,0:T(8,128)(2,1)} %bitcast.125), calls=%async_computation.2 | async-start | bytes 1048576 | tf_op jit(solution)/shard_map/all_to_all | solution.py:39
  85.3 7.7 %all-to-all-start.5 = ((bf16[4,16,512]{2,1,0:T(8,128)(2,1)}), bf16[4,16,512]{2,1,0:T(8,128)(2,1)S(1)}, u32[]{:S(2)}, u32[]{:S(2)}) async-start(bf16[4,16,512]{2,1,0:T(8,128)(2,1)} %bitcast.127), calls=%async_computation.5 | async-start | bytes 131072 | tf_op jit(solution)/shard_map/all_to_all | solution.py:39
  93.0 19.3 %all-to-all-start.3 = ((bf16[64,2,512]{2,1,0:T(2,128)(2,1)}), bf16[64,2,512]{2,1,0:T(2,128)(2,1)S(1)}, u32[]{:S(2)}, u32[]{:S(2)}) async-start(bf16[64,2,512]{2,1,0:T(2,128)(2,1)} %copy.111), calls=%async_computation.3 | async-start | bytes 262144 | tf_op jit(solution)/shard_map/all_to_all | solution.py:157
where the time goes:
time: 115 us; the launch traced here: 114 us
  waiting for transfers between devices  41 us (36%)
  starting transfers between devices  37.5 us (33%)
  matrix products  18.1 us (16%)
  local copies, waits for them, and re-layouts  13.4 us (12%)
  other arithmetic  3.7 us (3%)
    all_to_all x1, waiting for transfers between devices, shards(): lax.all_to_all(outbound, 'ep', split_axis=0, concat_axis=0, tiled=True)  14.4 us
    all_to_all x1, starting transfers between devices, shards(): lax.all_to_all(outbound, 'ep', split_axis=0, concat_axis=0, tiled=True)  13.8 us
    all_to_all x1, waiting for transfers between devices, shards(): lax.all_to_all(summed, 'ep', split_axis=0, concat_axis=0, tiled=True)  11.1 us
    all_to_all x2, waiting for transfers between devices, sent_and_summed(): lax.all_to_all(cut_along(shard, dim, devices), axis, 0, 0, tiled=True)  10.8 us
    all_to_all x1, starting transfers between devices, shards(): lax.all_to_all(summed, 'ep', split_axis=0, concat_axis=0, tiled=True)  8.19 us
    all_to_all x2, starting transfers between devices, from_everyone(): lax.all_to_all(jnp.broadcast_to(shard[None], (devices, *shard.shape)), ax...  8.05 us
    all_to_all x2, starting transfers between devices, sent_and_summed(): lax.all_to_all(cut_along(shard, dim, devices), axis, 0, 0, tiled=True)  7.48 us
    unnamed x29, local copies, waits for them, and re-layouts  6.66 us
  transfers between devices with their start and end apart: 6, of which 5 were waited for; matrix products, arithmetic and copies ran while one was open for 10% of the time, Pallas kernels for 0%

commit v1 on v0

v1 whole, which is shorter than its diff:
```python
import jax
import jax.numpy as jnp
from jax import lax
from jax.experimental import pallas as pl
from jax.experimental.pallas import tpu as pltpu
from jax.sharding import PartitionSpec as P

MESH = pl.DeviceIdType.MESH
BF = jnp.bfloat16
F32 = jnp.float32
EPS = 1e-06

SEQ = 16
D = 2048
QUARTER = 512
CACHE = 1024
NZ, NY, NC, NX = 8, 4, 2, 4
PEERS = NZ * NY * NC
ROWS = 2 * PEERS
ORDER = (0, 1, 7, 2, 6, 3, 5, 4)
PLACE = {dz: p for p, dz in enumerate(ORDER)}
CHUNKS = 4
CHUNK = ROWS // CHUNKS
GROUP = ROWS // NZ
BATCH = 4


def offsets(block):
    p, j = divmod(block, NY * NC)
    return ORDER[p], j // NC, j % NC


def opposite(block):
    dz, dy, dc = offsets(block)
    return PLACE[(NZ - dz) % NZ] * (NY * NC) + ((NY - dy) % NY) * NC + dc


def mm(a, b):
    return jnp.dot(a, b, preferred_element_type=F32)


def mm_t(a, b):
    return lax.dot_general(a, b, (((1,), (1,)), ((), ())), preferred_element_type=F32)


def silu(v):
    return v * (1.0 / (1.0 + jnp.exp(-v)))


def kernel(
    lambdas, lengths,
    tokens_h, norm_gain_h, wq_h, wk_h, wv_h, wo_h, head_gain_h, kc_h, vc_h, ffn_gain_h,
    routes_h, route_weight_h, eg_h, eu_h, ed_h, dg_h, du_h, dd_h, gate_h,
    out_ref,
    tok, ng, wq, wk, wv, wo, hg, kc, vc, fg, rt, rw, eg, eu, ed, dg, du, dd, gv,
    qs, own, nv, sc, ho, part1, ffn, outb, big, eparts, rs, rout, ret, dsend, drecv, gl, tick,
    load, kload, vload,
    p_send, p_recv, d_send, d_recv, ag_send, ag_recv, rs_send, rs_recv, b_send, b_recv,
    ds_send, ds_recv, g_send, g_recv,
):
    me = lax.axis_index("ep")
    x = lax.axis_index("tp")
    z, y, c = me // (NY * NC), (me // NC) % NY, me % NC

    def ep_at(block):
        dz, dy, dc = offsets(block)
        return ((z + dz) % NZ) * (NY * NC) + ((y + dy) % NY) * NC + (c + dc) % NC

    def messages(count, sem):
        size = tick.at[pl.ds(0, count)]
        pltpu.make_async_copy(size, size, sem).wait()

    loads = []

    def fetch(src, dst):
        copy = pltpu.make_async_copy(src, dst, load.at[len(loads)])
        copy.start()
        loads.append(copy)
        return copy

    l_tok = fetch(tokens_h, tok)
    l_ng = fetch(norm_gain_h, ng)
    l_wq = fetch(wq_h, wq)
    l_wk = fetch(wk_h, wk)
    l_wv = fetch(wv_h, wv)
    l_rt = fetch(routes_h, rt)
    l_rw = fetch(route_weight_h, rw)
    l_hg = fetch(head_gain_h, hg)
    l_fg = fetch(ffn_gain_h, fg)
    l_gv = fetch(gate_h, gv)
    for i in range(SEQ // BATCH):
        pltpu.make_async_copy(
            kc_h.at[pl.ds(i * BATCH, BATCH)], kc.at[pl.ds(i * BATCH, BATCH)], kload.at[i]
        ).start()
    for i in range(SEQ // BATCH):
        pltpu.make_async_copy(
            vc_h.at[pl.ds(i * BATCH, BATCH)], vc.at[pl.ds(i * BATCH, BATCH)], vload.at[i]
        ).start()
    l_wo = fetch(wo_h, wo)
    l_dg = fetch(dg_h, dg)
    l_du = fetch(du_h, du)
    l_dd = fetch(dd_h, dd)
    l_eg = fetch(eg_h, eg)
    l_eu = fetch(eu_h, eu)
    l_ed = fetch(ed_h, ed)

    barrier = pltpu.get_barrier_semaphore()

    @pl.loop(1, PEERS)
    def _(i):
        pl.semaphore_signal(barrier, inc=1, device_id=((me + i) % PEERS, x), device_id_type=MESH)

    @pl.loop(1, NX)
    def _(i):
        pl.semaphore_signal(barrier, inc=1, device_id=(me, (x + i) % NX), device_id_type=MESH)

    l_rt.wait()
    l_rw.wait()
    routes = rt[...]
    dz = ((routes >> 3) - z) & 7
    place = jnp.where(dz == 0, 0, jnp.where(dz <= 4, 2 * dz - 1, 16 - 2 * dz))
    dy = ((routes >> 1) - y) & 3
    dc = (routes - c) & 1
    rel = place * 8 + dy * 2 + dc
    row = lax.broadcasted_iota(jnp.int32, (ROWS, SEQ), 0)
    named = jnp.zeros((ROWS, SEQ), F32)
    weighted = jnp.zeros((ROWS, SEQ), F32)
    weights = rw[...]
    for k in range(4):
        hit = (row >> 1) == rel[k : k + 1, :]
        named = named + jnp.where(hit, 1.0, 0.0)
        weighted = weighted + jnp.where(hit, weights[k : k + 1, :], 0.0)
    before = lax.broadcasted_iota(jnp.int32, (SEQ, SEQ), 0) < lax.broadcasted_iota(
        jnp.int32, (SEQ, SEQ), 1
    )
    rank = mm(named.astype(BF), jnp.where(before, 1.0, 0.0).astype(BF))
    mine = jnp.abs(rank - (row & 1).astype(F32)) < 0.5
    dispatch = jnp.where(mine, named, 0.0).astype(BF)
    combine = jnp.where(mine, weighted, 0.0)

    l_tok.wait()
    l_ng.wait()
    wide = tok[...].astype(F32)
    scale = lax.rsqrt(jnp.mean(wide * wide, axis=-1, keepdims=True) + EPS)
    normed = (wide * scale * ng[...]).astype(BF)
    l_wq.wait()
    l_wk.wait()
    l_wv.wait()
    queries = mm(normed, wq[...]).astype(BF).astype(F32) * 0.125
    new_keys = mm(normed, wk[...]).astype(BF).astype(F32)
    nv[...] = mm(normed, wv[...]).astype(BF).astype(F32)
    low = lax.broadcasted_iota(jnp.int32, (SEQ, 128), 1) < 64
    for m in range(2):
        for g in range(2):
            head = queries[:, g * 128 : (g + 1) * 128]
            head = jnp.where(low, head, 0.0) if m == 0 else jnp.where(low, 0.0, head)
            r = (m * 2 + g) * SEQ
            qs[r : r + SEQ, :] = head
            score = jnp.sum(head * new_keys, axis=-1, keepdims=True)
            own[r : r + SEQ, :] = jnp.broadcast_to(score, (SEQ, 128))
    qs[4 * SEQ :, :] = jnp.zeros((4 * SEQ, 128), F32)
    own[4 * SEQ :, :] = jnp.zeros((4 * SEQ, 128), F32)

    @pl.loop(0, SEQ // BATCH)
    def _(i):
        pltpu.make_async_copy(
            kc_h.at[pl.ds(i * BATCH, BATCH)], kc.at[pl.ds(i * BATCH, BATCH)], kload.at[i]
        ).wait()
        for b in range(BATCH):
            s = i * BATCH + b
            q8 = qs[pl.ds(s, 8, stride=SEQ), :].astype(BF)
            sc[s] = mm_t(q8, kc[s])

    head_row = lax.broadcasted_iota(jnp.int32, (8, 1), 0)
    sign = jnp.where(head_row < 2, 1.0, jnp.where(head_row == 2, -lambdas[0], -lambdas[1]))
    sign = jnp.where(head_row < 4, sign, 0.0)
    position = lax.broadcasted_iota(jnp.int32, (8, CACHE), 1)

    @pl.loop(0, SEQ // BATCH)
    def _(i):
        pltpu.make_async_copy(
            vc_h.at[pl.ds(i * BATCH, BATCH)], vc.at[pl.ds(i * BATCH, BATCH)], vload.at[i]
        ).wait()
        for b in range(BATCH):
            s = i * BATCH + b
            scores = jnp.where(position < lengths[s], sc[s], -jnp.inf)
            own_score = own[pl.ds(s, 8, stride=SEQ), :][:, 0:1]
            top = jnp.maximum(jnp.max(scores, axis=-1, keepdims=True), own_score)
            probs = jnp.exp(scores - top)
            own_prob = jnp.exp(own_score - top)
            total = jnp.sum(probs, axis=-1, keepdims=True) + own_prob
            factor = sign / total
            probs = probs * factor
            own_prob = own_prob * factor
            attend = (probs + pltpu.roll(probs, 6, 0)).astype(BF)
            own_weight = (own_prob[0:2] + own_prob[2:4]).astype(BF).astype(F32)
            mixed = mm(attend, vc[s])[0:2] + own_weight * nv[pl.ds(s, 1), :]
            ho[pl.ds(s, 1), :] = mixed[0:1]
            ho[pl.ds(SEQ + s, 1), :] = mixed[1:2]

    l_hg.wait()
    heads = ho[...]
    heads = heads * lax.rsqrt(jnp.mean(heads * heads, axis=-1, keepdims=True) + EPS) * hg[...]
    heads = heads.astype(BF)
    l_wo.wait()
    part1[0] = (mm(heads[:SEQ], wo[0:128, :]) + mm(heads[SEQ:], wo[128:256, :])).astype(BF)

    pl.semaphore_wait(barrier, PEERS - 1 + NX - 1)

    def along_tp(r, src, dst, send, recv):
        return pltpu.make_async_remote_copy(
            src_ref=src, dst_ref=dst, send_sem=send, recv_sem=recv,
            device_id=(me, (x + r) % NX), device_id_type=MESH,
        )

    shares = []
    for r in (2, 1, 3):
        copy = along_tp(r, part1.at[0], part1.at[NX - r], p_send.at[r], p_recv.at[NX - r])
        copy.start()
        shares.append(copy)
    l_fg.wait()
    for r in (1, 3, 2):
        pltpu.make_async_copy(part1.at[r], part1.at[r], p_recv.at[r]).wait()
    total = part1[0].astype(F32)
    for r in (1, 2, 3):
        total = total + part1[r].astype(F32)
    residual = wide + total
    scale = lax.rsqrt(jnp.mean(residual * residual, axis=-1, keepdims=True) + EPS)
    ffn_in = (residual * scale * fg[...]).astype(BF)
    mine_at = pl.multiple_of(x * QUARTER, QUARTER)
    ffn[...] = ffn_in

    routed = mm(dispatch, ffn[:, pl.ds(mine_at, QUARTER)]).astype(BF)
    outb[...] = routed
    big[0, 0:2, :] = routed[0:2]
    for block in range(1, PEERS):
        there = opposite(block)
        pltpu.make_async_remote_copy(
            src_ref=outb.at[pl.ds(2 * block, 2), :],
            dst_ref=big.at[0, pl.ds(2 * there, 2), :],
            send_sem=d_send,
            recv_sem=d_recv.at[there // (NY * NC)],
            device_id=(ep_at(block), x),
            device_id_type=MESH,
        ).start()

    l_gv.wait()
    l_dg.wait()
    gate_pre = mm_t(ffn_in, dg[...])
    l_du.wait()
    hidden = (silu(gate_pre) * mm_t(ffn_in, du[...])).astype(BF)
    logit = jnp.sum(hidden.astype(F32) * gv[...], axis=-1, keepdims=True)
    gl[0] = jnp.broadcast_to(logit, (SEQ, 128))
    l_dd.wait()
    for r in range(NX):
        at = pl.multiple_of(((x + r) % NX) * QUARTER, QUARTER)
        dsend[r] = mm(hidden, dd[:, pl.ds(at, QUARTER)]).astype(BF)
    for r in (2, 1, 3):
        copy = along_tp(r, dsend.at[r], drecv.at[NX - r], ds_send.at[r], ds_recv.at[NX - r])
        copy.start()
        shares.append(copy)
        copy = along_tp(r, gl.at[0], gl.at[NX - r], g_send.at[r], g_recv.at[NX - r])
        copy.start()
        shares.append(copy)

    def arrived(ch):
        for p in (2 * ch, 2 * ch + 1):
            messages(GROUP // 2 - (p == 0), d_recv.at[p])
        rows = pl.ds(ch * CHUNK, CHUNK)
        for r in (2, 1, 3):
            copy = along_tp(
                r, big.at[0, rows, :], big.at[NX - r, rows, :],
                ag_send.at[ch, r], ag_recv.at[ch, NX - r],
            )
            copy.start()
            shares.append(copy)

    def work(ch):
        rows = pl.ds(ch * CHUNK, CHUNK)
        for r in (1, 3, 2):
            block = big.at[r, rows, :]
            pltpu.make_async_copy(block, block, ag_recv.at[ch, r]).wait()
        pre = jnp.zeros((CHUNK, 256), F32)
        up = jnp.zeros((CHUNK, 256), F32)
        for r in range(NX):
            at = pl.ds(pl.multiple_of(((x + r) % NX) * QUARTER, QUARTER), QUARTER)
            block = big[r, rows, :]
            pre = pre + mm(block, eg[at, :])
            up = up + mm(block, eu[at, :])
        hidden = (silu(pre) * up).astype(BF)
        for r in range(NX):
            at = pl.ds(pl.multiple_of(((x + r) % NX) * QUARTER, QUARTER), QUARTER)
            eparts[r, rows, :] = mm(hidden, ed[:, at]).astype(BF)
        for r in (2, 1, 3):
            copy = along_tp(
                r, eparts.at[r, rows, :], rs.at[NX - r, rows, :],
                rs_send.at[ch, r], rs_recv.at[ch, NX - r],
            )
            copy.start()
            shares.append(copy)

    def give_back(ch):
        rows = pl.ds(ch * CHUNK, CHUNK)
        for r in (1, 3, 2):
            block = rs.at[r, rows, :]
            pltpu.make_async_copy(block, block, rs_recv.at[ch, r]).wait()
        total = eparts[0, rows, :].astype(F32)
        for r in (1, 2, 3):
            total = total + rs[r, rows, :].astype(F32)
        total = total.astype(BF)
        rout[rows, :] = total
        if ch == 0:
            ret[0:2, :] = total[0:2]
        for block in range(ch * CHUNK // 2, (ch + 1) * CHUNK // 2):
            if block:
                pltpu.make_async_remote_copy(
                    src_ref=rout.at[pl.ds(2 * block, 2), :],
                    dst_ref=ret.at[pl.ds(2 * opposite(block), 2), :],
                    send_sem=b_send,
                    recv_sem=b_recv,
                    device_id=(ep_at(block), x),
                    device_id_type=MESH,
                ).start()

    arrived(0)
    arrived(1)
    l_eg.wait()
    l_eu.wait()
    l_ed.wait()
    arrived(2)
    arrived(3)
    work(1)
    work(2)
    give_back(1)
    work(3)
    give_back(2)
    work(0)
    give_back(3)
    give_back(0)

    for r in (1, 3, 2):
        pltpu.make_async_copy(drecv.at[r], drecv.at[r], ds_recv.at[r]).wait()
        pltpu.make_async_copy(gl.at[r], gl.at[r], g_recv.at[r]).wait()
    dense = dsend[0].astype(F32)
    logit = gl[0]
    for r in (1, 2, 3):
        dense = dense + drecv[r].astype(F32)
        logit = logit + gl[r]
    gate = 1.0 / (1.0 + jnp.exp(-logit[:, 0:1]))
    kept = tok[:, pl.ds(mine_at, QUARTER)].astype(F32)
    for r in range(NX):
        kept = kept + part1[r, :, pl.ds(mine_at, QUARTER)].astype(F32)
    kept = kept + gate * dense
    coarse = combine.astype(BF)
    fine = (combine - coarse.astype(F32)).astype(BF)

    messages(PEERS - 1, b_recv)
    back = ret[...]
    over = (((0,), (0,)), ((), ()))
    mix = lax.dot_general(coarse, back, over, preferred_element_type=F32)
    mix = mix + lax.dot_general(fine, back, over, preferred_element_type=F32)
    out_ref[...] = (kept + mix).astype(BF)

    for copy in shares:
        copy.wait_send()
    messages(PEERS - 1, d_send)
    messages(PEERS - 1, b_send)


def shards(
    tokens, norm_gain, query_weight, key_weight, value_weight, output_weight, head_gain, lambdas,
    key_cache, value_cache, lengths, ffn_gain, routes, route_weight, expert_gate, expert_up,
    expert_down, dense_gate, dense_up, dense_down, gate_vector,
):
    hbm = pl.BlockSpec(memory_space=pl.ANY)
    smem = pl.BlockSpec(memory_space=pltpu.SMEM)
    vm = pltpu.VMEM
    dma = pltpu.SemaphoreType.DMA
    return pl.pallas_call(
        kernel,
        name="layer",
        out_shape=jax.ShapeDtypeStruct((SEQ, QUARTER), BF),
        in_specs=[smem, smem] + [hbm] * 19,
        out_specs=pl.BlockSpec(memory_space=pltpu.VMEM),
        scratch_shapes=[
            vm((SEQ, D), BF), vm((1, D), F32), vm((D, 256), BF), vm((D, 128), BF), vm((D, 128), BF),
            vm((256, D), BF), vm((1, 128), F32), vm((SEQ, CACHE, 128), BF), vm((SEQ, CACHE, 128), BF),
            vm((1, D), F32), vm((4, SEQ), jnp.int32), vm((4, SEQ), F32),
            vm((D, 256), BF), vm((D, 256), BF), vm((256, D), BF),
            vm((512, D), BF), vm((512, D), BF), vm((512, D), BF), vm((1, 512), F32),
            vm((8 * SEQ, 128), F32), vm((8 * SEQ, 128), F32), vm((SEQ, 128), F32),
            vm((SEQ, 8, CACHE), F32), vm((2 * SEQ, 128), F32),
            vm((NX, SEQ, D), BF), vm((SEQ, D), BF), vm((ROWS, QUARTER), BF),
            vm((NX, ROWS, QUARTER), BF), vm((NX, ROWS, QUARTER), BF), vm((NX, ROWS, QUARTER), BF),
            vm((ROWS, QUARTER), BF), vm((ROWS, QUARTER), BF),
            vm((NX, SEQ, QUARTER), BF), vm((NX, SEQ, QUARTER), BF), vm((NX, SEQ, 128), F32),
            vm((PEERS, 8, 128), BF),
            dma((17,)), dma((SEQ // BATCH,)), dma((SEQ // BATCH,)),
            dma((NX,)), dma((NX,)), dma, dma((NZ,)), dma((CHUNKS, NX)), dma((CHUNKS, NX)),
            dma((CHUNKS, NX)), dma((CHUNKS, NX)), dma, dma,
            dma((NX,)), dma((NX,)), dma((NX,)), dma((NX,)),
        ],
        compiler_params=pltpu.CompilerParams(
            collective_id=0, has_side_effects=True, vmem_limit_bytes=60 * 1024 * 1024
        ),
    )(
        lambdas, lengths,
        tokens, norm_gain.reshape(1, D), query_weight, key_weight, value_weight, output_weight,
        head_gain.reshape(1, 128), key_cache.reshape(SEQ, CACHE, 128),
        value_cache.reshape(SEQ, CACHE, 128), ffn_gain.reshape(1, D),
        routes.T, route_weight.T,
        expert_gate.reshape(D, 256), expert_up.reshape(D, 256), expert_down.reshape(256, D),
        dense_gate, dense_up, dense_down, gate_vector.reshape(1, 512),
    )


def solution(mesh):
    placed = (
        P("ep", None), P(), P(None, "tp"), P(None, "tp"), P(None, "tp"), P("tp", None), P(), P("tp"),
        P("ep", None, "tp", None), P("ep", None, "tp", None), P("ep"), P(), P("ep", None),
        P("ep", None), P("ep", None, "tp"), P("ep", None, "tp"), P("ep", "tp", None),
        P("tp", None), P("tp", None), P("tp", None), P("tp"),
    )
    return jax.shard_map(
        shards, mesh=mesh, in_specs=placed, out_specs=P("ep", "tp"), check_vma=False
    )
```

time: 115 us -> 52 us (0.45)
  Pallas kernels: 0 us -> 50.4 us
  waiting for transfers between devices: 41 us -> 0 us
  starting transfers between devices: 37.5 us -> 0 us
  matrix products: 18.1 us -> 0 us
  local copies, waits for them, and re-layouts: 13.4 us -> 1.32 us
  other arithmetic: 3.7 us -> 0 us
    pallas_call x0 -> x1, Pallas kernels: none -> 50.4 us  [shards(): pl.pallas_call(kernel, name='layer', out_shape=jax.ShapeDtypeStruct((SEQ,...]
    all_to_all x6 -> x0, waiting for transfers between devices: 41 us -> none  [the longest x1 14.4 us: shards(): lax.all_to_all(outbound, 'ep', split_axis=0, concat_axis=0, tiled=True)]
    all_to_all x6 -> x0, starting transfers between devices: 37.5 us -> none  [the longest x1 13.8 us: shards(): lax.all_to_all(outbound, 'ep', split_axis=0, concat_axis=0, tiled=True)]
    dot_general x14 -> x0, matrix products: 18.1 us -> none  [the longest x1 3.06 us: shards(): jnp.einsum('skgc,sckv->skgv', cache_weight, value_cache, preferred_elemen...]
    unnamed x29 -> x1, local copies, waits for them, and re-layouts: 6.66 us -> 1.32 us
    reshape x5 -> x0, local copies, waits for them, and re-layouts: 2.85 us -> none  [the longest x2 1.47 us: cut_along(): return jnp.moveaxis(shard.reshape(*before, devices, -1, *after), dim, 0)]
    reduce_sum x10 -> x0, other arithmetic: 2.14 us -> none  [the longest x2 1.25 us: rms_scale(): jnp.mean(values * values, axis=-1, keepdims=True) + epsilon]
    broadcast_in_dim x2 -> x0, local copies, waits for them, and re-layouts: 1.3 us -> none  [from_everyone(): jnp.broadcast_to(shard[None], (devices, *shard.shape))]
  transfers between devices with their start and end apart: 6 -> 0, of which waited for: 5 -> 0; matrix products, arithmetic and copies ran while one was open for 10% -> 0% of each run, Pallas kernels for 0% -> 0%
where the time goes in v1:
time: 52 us; the launch traced here: 51.8 us
  Pallas kernels  50.4 us (97%)
  local copies, waits for them, and re-layouts  1.32 us (3%)
    pallas_call x1, Pallas kernels, shards(): pl.pallas_call(kernel, name='layer', out_shape=jax.ShapeDtypeStruct((SEQ,...  50.4 us
    unnamed x1, local copies, waits for them, and re-layouts  1.32 us

profile of v1, /device:TPU:1, one launch (start us, length us, event | category | flops | bytes accessed | tf_op | source)
XLA Modules:
  0.0 51.8 jit_solution(17100587592057152844)
XLA Ops:
  0.0 50.4 %layer.1 = bf16[16,512]{1,0:T(8,128)(2,1)} custom-call(f32[2]{0:T(128)} %lambdas.1, s32[16]{0:T(128)} %lengths.1, bf16[16,2048]{1,0:T(8,128)(2,1)} %tokens_h.1, f32[1,2048]{1,0:T(1,128)} %bitcast.16, bf16[2048,256]{1,0:T(8,128)(2,1)} %wq_h.1, bf16[2048,128]{1,0:T(8,128)(2,1)} %wk_h.1, bf16[2048,128]{1,0:T(8,128)(2,1)} %wv_h.1, bf16[256,2048]{1,0:T(8,128)(2,1)} %wo_h.1, ...), custom_call_target="tpu_custom_call" | custom-call | tf_op jit(solution)/shard_map/layer/pallas_call | solution.py:379
  50.4 1.3 %copy.23 = bf16[16,512]{1,0:T(8,128)(2,1)} copy(bf16[16,512]{1,0:T(8,128)(2,1)} %layer.1) | data formatting | bytes 32768

commit v2 on v1

v2 whole, which is shorter than its diff:
```python
import jax
import jax.numpy as jnp
from jax import lax
from jax.experimental import pallas as pl
from jax.experimental.pallas import tpu as pltpu
from jax.sharding import PartitionSpec as P

MESH = pl.DeviceIdType.MESH
BF = jnp.bfloat16
F32 = jnp.float32
EPS = 1e-06

SEQ = 16
D = 2048
QUARTER = 512
CACHE = 1024
NZ, NY, NC, NX = 8, 4, 2, 4
PEERS = NZ * NY * NC
ROWS = 2 * PEERS
ORDER = (0, 1, 7, 2, 6, 3, 5, 4)
PLACE = {dz: p for p, dz in enumerate(ORDER)}
CHUNKS = 4
CHUNK = ROWS // CHUNKS
GROUP = ROWS // NZ
BATCH = 4
HELD = (0, 2, 1, 3)
SWAPPED = ((0, 1, 1, 0), (0, 0, 1, 1))


def offsets(block):
    p, j = divmod(block, NY * NC)
    return ORDER[p], j // NC, j % NC


def opposite(block):
    dz, dy, dc = offsets(block)
    return PLACE[(NZ - dz) % NZ] * (NY * NC) + ((NY - dy) % NY) * NC + dc


def mm(a, b):
    return jnp.dot(a, b, preferred_element_type=F32)


def mm_t(a, b):
    return lax.dot_general(a, b, (((1,), (1,)), ((), ())), preferred_element_type=F32)


def silu(v):
    return v * (1.0 / (1.0 + jnp.exp(-v)))


def kernel(
    lambdas_h, lengths_h,
    tokens_h, norm_gain_h, wq_h, wk_h, wv_h, wo_h, head_gain_h, kc_h, vc_h, ffn_gain_h,
    routes_h, route_weight_h, eg_h, eu_h, ed_h, dg_h, du_h, dd_h, gate_h,
    out_ref,
    lambdas, lengths,
    tok, ng, wq, wk, wv, wo, hg, kc, vc, fg, rt, rw, eg, eu, ed, dg, du, dd, gv,
    qs, own, nv, sc, at, ho, near, far, ffn, outb, big, ungain,
    eparts, rs, rout, ret, ret2, dsend, drecv, gl, tick,
    load,
    p_send, p_recv, d_send, d_recv, ag_send, ag_recv, rs_send, rs_recv,
    b_send, b_recv, o_send, o_recv, ds_send, ds_recv, g_send, g_recv,
):
    me = lax.axis_index("ep")
    x = lax.axis_index("tp")
    z = lax.div(me, NY * NC)
    y = lax.rem(lax.div(me, NC), NY)
    c = lax.rem(me, NC)
    tps = [lax.rem(x + r, NX) for r in range(NX)]
    zs = [lax.rem(z + dz, NZ) * (NY * NC) for dz in range(NZ)]
    yc = [lax.rem(y + j // NC, NY) * NC + lax.rem(c + j % NC, NC) for j in range(NY * NC)]

    def ep_at(block):
        p, j = divmod(block, NY * NC)
        return zs[ORDER[p]] + yc[j]

    def quarter(r):
        return pl.ds(pl.multiple_of(tps[r] * QUARTER, QUARTER), QUARTER)

    def columns(r):
        return pl.ds(HELD.index(r) * QUARTER, QUARTER)

    def messages(count, sem):
        size = tick.at[pl.ds(0, count)]
        pltpu.make_async_copy(size, size, sem).wait()

    loads = []

    def fetch(src, dst):
        copy = pltpu.make_async_copy(src, dst, load.at[len(loads)])
        copy.start()
        loads.append(copy)
        return copy

    l_tok = fetch(tokens_h, tok)
    l_ng = fetch(norm_gain_h, ng)
    l_wq = fetch(wq_h, wq)
    l_wk = fetch(wk_h, wk)
    l_wv = fetch(wv_h, wv)
    parts = [pl.ds(i * BATCH, BATCH) for i in range(SEQ // BATCH)]
    keys = [fetch(kc_h.at[part], kc.at[part]) for part in parts]
    l_small = [
        fetch(lambdas_h, lambdas), fetch(lengths_h, lengths), fetch(head_gain_h, hg),
        fetch(ffn_gain_h, fg), fetch(routes_h, rt), fetch(route_weight_h, rw), fetch(gate_h, gv),
    ]
    values = [fetch(vc_h.at[part], vc.at[part]) for part in parts]
    l_wo = fetch(wo_h, wo)

    barrier = pltpu.get_barrier_semaphore()
    for r in (1, 2, 3):
        pl.semaphore_signal(barrier, inc=1, device_id=(me, tps[r]), device_id_type=MESH)
    for block in range(1, PEERS):
        there = ep_at(block)
        pl.semaphore_signal(barrier, inc=1, device_id=(there, x), device_id_type=MESH)
        pl.semaphore_signal(barrier, inc=1, device_id=(there, tps[2]), device_id_type=MESH)

    qs[...] = jnp.zeros((8 * SEQ, 128), F32)
    own[...] = jnp.zeros((8 * SEQ, 128), F32)
    l_tok.wait()
    l_ng.wait()
    wide = tok[...].astype(F32)
    scale = lax.rsqrt(jnp.mean(wide * wide, axis=-1, keepdims=True) + EPS)
    normed = (wide * scale * ng[...]).astype(BF)
    l_wq.wait()
    l_wk.wait()
    l_wv.wait()
    queries = mm(normed, wq[...]).astype(BF).astype(F32) * 0.125
    new_keys = mm(normed, wk[...]).astype(BF).astype(F32)
    nv[...] = mm(normed, wv[...]).astype(BF).astype(F32)
    low = lax.broadcasted_iota(jnp.int32, (SEQ, 128), 1) < 64
    even = (lax.broadcasted_iota(jnp.int32, (SEQ, 128), 0) & 1) == 0
    for m in range(2):
        for g in range(2):
            head = queries[:, g * 128 : (g + 1) * 128]
            head = jnp.where(low, head, 0.0) if m == 0 else jnp.where(low, 0.0, head)
            score = jnp.sum(head * new_keys, axis=-1, keepdims=True)
            score = jnp.broadcast_to(score, (SEQ, 128))
            for odd in range(2):
                r = (odd * 4 + m * 2 + g) * SEQ
                keep = jnp.logical_not(even) if odd else even
                qs[r : r + SEQ, :] = jnp.where(keep, head, 0.0)
                own[r : r + SEQ, :] = jnp.where(keep, score, 0.0)

    def of(ref, i):
        return ref[pl.ds(i, 8, stride=SEQ), :]

    for i in range(0, SEQ, 2):
        if i % BATCH == 0:
            keys[i // BATCH].wait()
        pair = mm_t(of(qs, i).astype(BF), kc[i])
        sc[i // 2] = pair + mm_t(of(qs, i + 1).astype(BF), kc[i + 1])
    l_dg = fetch(dg_h, dg)
    l_du = fetch(du_h, du)
    l_dd = fetch(dd_h, dd)
    l_eg = fetch(eg_h, eg)
    l_eu = fetch(eu_h, eu)
    l_ed = fetch(ed_h, ed)

    for copy in l_small:
        copy.wait()
    head_row = lax.broadcasted_iota(jnp.int32, (8, 1), 0)
    turn = head_row & 3
    sign = jnp.where(turn < 2, 1.0, jnp.where(turn == 2, -lambdas[0], -lambdas[1]))
    position = lax.broadcasted_iota(jnp.int32, (8, CACHE), 1)
    own_weights = []
    for i in range(0, SEQ, 2):
        live = jnp.where(head_row < 4, lengths[i], lengths[i + 1])
        scores = jnp.where(position < live, sc[i // 2], -jnp.inf)
        own_score = (of(own, i) + of(own, i + 1))[:, 0:1]
        top = jnp.maximum(jnp.max(scores, axis=-1, keepdims=True), own_score)
        probs = jnp.exp(scores - top)
        own_prob = jnp.exp(own_score - top)
        factor = sign / (jnp.sum(probs, axis=-1, keepdims=True) + own_prob)
        probs = probs * factor
        own_prob = own_prob * factor
        at[i // 2] = (probs + pltpu.roll(probs, 6, 0)).astype(BF)
        for first in (0, 4):
            both = own_prob[first : first + 2] + own_prob[first + 2 : first + 4]
            own_weights.append(both.astype(BF).astype(F32))

    for i in range(SEQ):
        if i % BATCH == 0:
            values[i // BATCH].wait()
        first = 4 * (i % 2)
        mixed = mm(at[i // 2], vc[i])[first : first + 2] + own_weights[i] * nv[i : i + 1, :]
        ho[i : i + 1, :] = mixed[0:1]
        ho[SEQ + i : SEQ + i + 1, :] = mixed[1:2]

    heads = ho[...]
    heads = heads * lax.rsqrt(jnp.mean(heads * heads, axis=-1, keepdims=True) + EPS) * hg[...]
    heads = heads.astype(BF)
    l_wo.wait()
    for ref, held in ((far, (1, 3)), (near, (0, 2))):
        for i, r in enumerate(held):
            share = mm(heads[:SEQ], wo[0:128, quarter(r)]) + mm(heads[SEQ:], wo[128:256, quarter(r)])
            ref[0, :, i * QUARTER : (i + 1) * QUARTER] = share.astype(BF)

    pl.semaphore_wait(barrier, 2 * (PEERS - 1) + NX - 1)

    def along_tp(r, src, dst, send, recv):
        return pltpu.make_async_remote_copy(
            src_ref=src, dst_ref=dst, send_sem=send, recv_sem=recv,
            device_id=(me, tps[r]), device_id_type=MESH,
        )

    shares = []

    def share_out(turn, r, src, dst):
        copy = along_tp(
            r, src.at[0], dst.at[NX - r], p_send.at[turn, r], p_recv.at[turn, NX - r]
        )
        copy.start()
        shares.append(copy)

    share_out(0, 1, far, near)
    share_out(0, 3, far, near)
    share_out(0, 2, near, near)
    share_out(1, 1, near, far)
    share_out(1, 3, near, far)
    share_out(1, 2, far, far)

    for r in HELD:
        ungain[:, columns(r)] = 1.0 / fg[:, quarter(r)]
    routes = rt[...]
    dz = ((routes >> 3) - z) & 7
    place = jnp.where(dz == 0, 0, jnp.where(dz <= 4, 2 * dz - 1, 16 - 2 * dz))
    dy = ((routes >> 1) - y) & 3
    dc = (routes - c) & 1
    rel = place * 8 + dy * 2 + dc
    row = lax.broadcasted_iota(jnp.int32, (ROWS, SEQ), 0)
    named = jnp.zeros((ROWS, SEQ), F32)
    weighted = jnp.zeros((ROWS, SEQ), F32)
    weights = rw[...]
    for k in range(4):
        hit = (row >> 1) == rel[k : k + 1, :]
        named = named + jnp.where(hit, 1.0, 0.0)
        weighted = weighted + jnp.where(hit, weights[k : k + 1, :], 0.0)
    before = lax.broadcasted_iota(jnp.int32, (SEQ, SEQ), 0) < lax.broadcasted_iota(
        jnp.int32, (SEQ, SEQ), 1
    )
    rank = mm(named.astype(BF), jnp.where(before, 1.0, 0.0).astype(BF))
    mine = jnp.abs(rank - (row & 1).astype(F32)) < 0.5
    dispatch = jnp.where(mine, named, 0.0).astype(BF)
    combine = jnp.where(mine, weighted, 0.0)

    def arrived_share(turn, ref, held):
        for r in (1, 3, 2):
            block = ref.at[r]
            pltpu.make_async_copy(block, block, p_recv.at[turn, r]).wait()
        half = []
        for i, r in enumerate(held):
            total = tok[:, quarter(r)].astype(F32)
            for sender in range(NX):
                swapped = SWAPPED[turn][sender]
                j = 1 - i if swapped else i
                total = total + ref[sender, :, j * QUARTER : (j + 1) * QUARTER].astype(F32)
            half.append(total)
            ffn[:, columns(r)] = (total * fg[:, quarter(r)]).astype(BF)
        return half

    first_half = arrived_share(0, near, (0, 2))
    outb[...] = mm(dispatch, ffn[:, 0 : 2 * QUARTER]).astype(BF)
    big[0:2, 0 : 2 * QUARTER] = outb[0:2, :]
    for block in reversed(range(1, PEERS)):
        there = opposite(block)
        pltpu.make_async_remote_copy(
            src_ref=outb.at[pl.ds(2 * block, 2), :],
            dst_ref=big.at[pl.ds(2 * there, 2), pl.ds(0, 2 * QUARTER)],
            send_sem=d_send,
            recv_sem=d_recv.at[there // (NY * NC)],
            device_id=(ep_at(block), x),
            device_id_type=MESH,
        ).start()

    second_half = arrived_share(1, far, (1, 3))
    squares = jnp.zeros((SEQ, 1), F32)
    for value in first_half + second_half:
        squares = squares + jnp.sum(value * value, axis=-1, keepdims=True)
    scale = lax.rsqrt(squares * (1.0 / D) + EPS)
    l_dg.wait()
    l_du.wait()
    pre = jnp.zeros((SEQ, 512), F32)
    up = jnp.zeros((SEQ, 512), F32)
    for r in HELD:
        block = ffn[:, columns(r)]
        pre = pre + mm_t(block, dg[:, quarter(r)])
        up = up + mm_t(block, du[:, quarter(r)])
    hidden = (silu(pre * scale) * (up * scale)).astype(BF)
    logit = jnp.sum(hidden.astype(F32) * gv[...], axis=-1, keepdims=True)
    gl[0] = jnp.broadcast_to(logit, (SEQ, 128))
    l_dd.wait()
    for r in range(NX):
        dsend[r] = mm(hidden, dd[:, quarter(r)]).astype(BF)
    for r in (2, 1, 3):
        copy = along_tp(r, dsend.at[r], drecv.at[NX - r], ds_send.at[r], ds_recv.at[NX - r])
        copy.start()
        shares.append(copy)
        copy = along_tp(r, gl.at[0], gl.at[NX - r], g_send.at[r], g_recv.at[NX - r])
        copy.start()
        shares.append(copy)

    def arrived(ch):
        for p in (2 * ch + 1, 2 * ch):
            messages(2 * GROUP - 4 * (p == 0), d_recv.at[p])
        rows = pl.ds(ch * CHUNK, CHUNK)
        for r in (1, 3):
            copy = along_tp(
                r, big.at[rows, columns(0)], big.at[rows, columns(NX - r)],
                ag_send.at[ch, r], ag_recv.at[ch, NX - r],
            )
            copy.start()
            shares.append(copy)

    def work(ch):
        rows = pl.ds(ch * CHUNK, CHUNK)
        for r in (1, 3):
            block = big.at[rows, columns(r)]
            pltpu.make_async_copy(block, block, ag_recv.at[ch, r]).wait()
        pre = jnp.zeros((CHUNK, 256), F32)
        up = jnp.zeros((CHUNK, 256), F32)
        squares = jnp.zeros((CHUNK, QUARTER), F32)
        for r in HELD:
            block = big[rows, columns(r)]
            pre = pre + mm(block, eg[quarter(r), :])
            up = up + mm(block, eu[quarter(r), :])
            value = block.astype(F32) * ungain[:, columns(r)]
            squares = squares + value * value
        row_scale = jnp.sum(squares, axis=-1, keepdims=True) * (1.0 / D)
        row_scale = lax.rsqrt(row_scale + EPS)
        hidden = (silu(pre * row_scale) * (up * row_scale)).astype(BF)
        for r in (1, 3, 2, 0):
            eparts[r, rows, :] = mm(hidden, ed[:, quarter(r)]).astype(BF)
        for r in (1, 3):
            copy = along_tp(
                r, eparts.at[r, rows, :], rs.at[NX - r, rows, :],
                rs_send.at[ch, r], rs_recv.at[ch, NX - r],
            )
            copy.start()
            shares.append(copy)

    def send_rows(src, dst, send, recv, tp, blocks):
        for block in reversed(blocks):
            pltpu.make_async_remote_copy(
                src_ref=src.at[pl.ds(2 * block, 2), :],
                dst_ref=dst.at[pl.ds(2 * opposite(block), 2), :],
                send_sem=send,
                recv_sem=recv,
                device_id=(ep_at(block), tp),
                device_id_type=MESH,
            ).start()

    def give_back(ch):
        rows = pl.ds(ch * CHUNK, CHUNK)
        total = eparts[0, rows, :].astype(F32)
        for r in (1, 3):
            block = rs.at[r, rows, :]
            pltpu.make_async_copy(block, block, rs_recv.at[ch, r]).wait()
            total = total + rs[r, rows, :].astype(F32)
        total = total.astype(BF)
        rout[rows, :] = total
        if ch == 0:
            ret[0:2, :] = total[0:2]
        send_rows(rout, ret, b_send, b_recv, x, range(max(1, ch * CHUNK // 2), (ch + 1) * CHUNK // 2))

    arrived(3)
    arrived(2)
    arrived(1)
    arrived(0)
    l_eg.wait()
    l_eu.wait()
    l_ed.wait()
    work(3)
    work(2)
    work(1)
    work(0)
    send_rows(eparts.at[2], ret2, o_send, o_recv, tps[2], range(PEERS))
    give_back(3)
    give_back(2)
    give_back(1)
    give_back(0)

    for r in (1, 3, 2):
        pltpu.make_async_copy(drecv.at[r], drecv.at[r], ds_recv.at[r]).wait()
        pltpu.make_async_copy(gl.at[r], gl.at[r], g_recv.at[r]).wait()
    dense = dsend[0].astype(F32)
    logit = gl[0]
    for r in (1, 2, 3):
        dense = dense + drecv[r].astype(F32)
        logit = logit + gl[r]
    gate = 1.0 / (1.0 + jnp.exp(-logit[:, 0:1]))
    kept = first_half[0] + gate * dense
    coarse = combine.astype(BF)
    fine = (combine - coarse.astype(F32)).astype(BF)

    messages(2 * PEERS, o_recv)
    messages(2 * PEERS - 2, b_recv)
    back = (ret[...].astype(F32) + ret2[...].astype(F32)).astype(BF)
    over = (((0,), (0,)), ((), ()))
    mix = lax.dot_general(coarse, back, over, preferred_element_type=F32)
    mix = mix + lax.dot_general(fine, back, over, preferred_element_type=F32)
    out_ref[...] = (kept + mix).astype(BF)

    for copy in shares:
        copy.wait_send()
    messages(4 * PEERS - 4, d_send)
    messages(2 * PEERS - 2, b_send)
    messages(2 * PEERS, o_send)


def shards(
    tokens, norm_gain, query_weight, key_weight, value_weight, output_weight, head_gain, lambdas,
    key_cache, value_cache, lengths, ffn_gain, routes, route_weight, expert_gate, expert_up,
    expert_down, dense_gate, dense_up, dense_down, gate_vector,
):
    hbm = pl.BlockSpec(memory_space=pl.ANY)
    vm = pltpu.VMEM
    dma = pltpu.SemaphoreType.DMA
    return pl.pallas_call(
        kernel,
        name="layer",
        out_shape=jax.ShapeDtypeStruct((SEQ, QUARTER), BF),
        in_specs=[hbm] * 21,
        out_specs=pl.BlockSpec(memory_space=pltpu.VMEM),
        scratch_shapes=[
            pltpu.SMEM((2,), F32), pltpu.SMEM((SEQ,), jnp.int32),
            vm((SEQ, D), BF), vm((1, D), F32), vm((D, 256), BF), vm((D, 128), BF), vm((D, 128), BF),
            vm((256, D), BF), vm((1, 128), F32), vm((SEQ, CACHE, 128), BF), vm((SEQ, CACHE, 128), BF),
            vm((1, D), F32), vm((4, SEQ), jnp.int32), vm((4, SEQ), F32),
            vm((D, 256), BF), vm((D, 256), BF), vm((256, D), BF),
            vm((512, D), BF), vm((512, D), BF), vm((512, D), BF), vm((1, 512), F32),
            vm((8 * SEQ, 128), F32), vm((8 * SEQ, 128), F32), vm((SEQ, 128), F32),
            vm((SEQ // 2, 8, CACHE), F32), vm((SEQ // 2, 8, CACHE), BF), vm((2 * SEQ, 128), F32),
            vm((NX, SEQ, 2 * QUARTER), BF), vm((NX, SEQ, 2 * QUARTER), BF), vm((SEQ, D), BF),
            vm((ROWS, 2 * QUARTER), BF), vm((ROWS, D), BF), vm((1, D), F32),
            vm((NX, ROWS, QUARTER), BF), vm((NX, ROWS, QUARTER), BF),
            vm((ROWS, QUARTER), BF), vm((ROWS, QUARTER), BF), vm((ROWS, QUARTER), BF),
            vm((NX, SEQ, QUARTER), BF), vm((NX, SEQ, QUARTER), BF), vm((NX, SEQ, 128), F32),
            vm((4 * PEERS, 2, 128), F32),
            dma((27,)),
            dma((2, NX)), dma((2, NX)), dma, dma((NZ,)),
            dma((CHUNKS, NX)), dma((CHUNKS, NX)), dma((CHUNKS, NX)), dma((CHUNKS, NX)),
            dma, dma, dma, dma, dma((NX,)), dma((NX,)), dma((NX,)), dma((NX,)),
        ],
        compiler_params=pltpu.CompilerParams(
            collective_id=0, has_side_effects=True, vmem_limit_bytes=60 * 1024 * 1024
        ),
    )(
        lambdas, lengths,
        tokens, norm_gain.reshape(1, D), query_weight, key_weight, value_weight, output_weight,
        head_gain.reshape(1, 128), key_cache.reshape(SEQ, CACHE, 128),
        value_cache.reshape(SEQ, CACHE, 128), ffn_gain.reshape(1, D),
        routes.T, route_weight.T,
        expert_gate.reshape(D, 256), expert_up.reshape(D, 256), expert_down.reshape(256, D),
        dense_gate, dense_up, dense_down, gate_vector.reshape(1, 512),
    )


def solution(mesh):
    placed = (
        P("ep", None), P(), P(None, "tp"), P(None, "tp"), P(None, "tp"), P("tp", None), P(), P("tp"),
        P("ep", None, "tp", None), P("ep", None, "tp", None), P("ep"), P(), P("ep", None),
        P("ep", None), P("ep", None, "tp"), P("ep", None, "tp"), P("ep", "tp", None),
        P("tp", None), P("tp", None), P("tp", None), P("tp"),
    )
    return jax.shard_map(
        shards, mesh=mesh, in_specs=placed, out_specs=P("ep", "tp"), check_vma=False
    )
```

time: 52 us -> 44.5 us (0.86)
  Pallas kernels: 50.4 us -> 43 us
    pallas_call x1, Pallas kernels: 50.4 us -> 43 us  [shards(): pl.pallas_call(kernel, name='layer', out_shape=jax.ShapeDtypeStruct((SEQ,...]
where the time goes in v2:
time: 44.5 us; the launch traced here: 44.4 us
  Pallas kernels  43 us (97%)
  local copies, waits for them, and re-layouts  1.32 us (3%)
    pallas_call x1, Pallas kernels, shards(): pl.pallas_call(kernel, name='layer', out_shape=jax.ShapeDtypeStruct((SEQ,...  43 us
    unnamed x1, local copies, waits for them, and re-layouts  1.32 us

profile of v2, /device:TPU:1, one launch (start us, length us, event | category | flops | bytes accessed | tf_op | source)
XLA Modules:
  0.0 44.4 jit_solution(7262699334125487887)
XLA Ops:
  0.0 43.0 %layer.1 = bf16[16,512]{1,0:T(8,128)(2,1)} custom-call(f32[2]{0:T(128)} %lambdas_h.1, s32[16]{0:T(128)} %lengths_h.1, bf16[16,2048]{1,0:T(8,128)(2,1)} %tokens_h.1, f32[1,2048]{1,0:T(1,128)} %bitcast.16, bf16[2048,256]{1,0:T(8,128)(2,1)} %wq_h.1, bf16[2048,128]{1,0:T(8,128)(2,1)} %wk_h.1, bf16[2048,128]{1,0:T(8,128)(2,1)} %wv_h.1, bf16[256,2048]{1,0:T(8,128)(2,1)} %wo_h.1, ...), custom_call_target="tpu_custom_call" | custom-call | tf_op jit(solution)/shard_map/layer/pallas_call | solution.py:419
  43.0 1.3 %copy.23 = bf16[16,512]{1,0:T(8,128)(2,1)} copy(bf16[16,512]{1,0:T(8,128)(2,1)} %layer.1) | data formatting | bytes 32768

commit v3 on v2

--- a/solution.py
+++ b/solution.py
@@ -23,6 +23,8 @@
 CHUNK = ROWS // CHUNKS
 GROUP = ROWS // NZ
 BATCH = 4
+DIRECT = (True, True, True, False)
+PARTNERS = {True: (1, 3), False: (2, 1, 3)}
 HELD = (0, 2, 1, 3)
 SWAPPED = ((0, 1, 1, 0), (0, 0, 1, 1))
 
@@ -35,6 +37,10 @@
 def opposite(block):
     dz, dy, dc = offsets(block)
     return PLACE[(NZ - dz) % NZ] * (NY * NC) + ((NY - dy) % NY) * NC + dc
+
+
+def chunk_of(block):
+    return 2 * block // CHUNK
 
 
 def mm(a, b):
@@ -107,10 +113,14 @@
     values = [fetch(vc_h.at[part], vc.at[part]) for part in parts]
     l_wo = fetch(wo_h, wo)
 
+    for p in range(NZ):
+        if not DIRECT[chunk_of(opposite(p * NY * NC))]:
+            ret2[p * GROUP : (p + 1) * GROUP, :] = jnp.zeros((GROUP, QUARTER), BF)
+
     barrier = pltpu.get_barrier_semaphore()
     for r in (1, 2, 3):
         pl.semaphore_signal(barrier, inc=1, device_id=(me, tps[r]), device_id_type=MESH)
-    for block in range(1, PEERS):
+    for block in reversed(range(1, PEERS)):
         there = ep_at(block)
         pl.semaphore_signal(barrier, inc=1, device_id=(there, x), device_id_type=MESH)
         pl.semaphore_signal(barrier, inc=1, device_id=(there, tps[2]), device_id_type=MESH)
@@ -264,9 +274,10 @@
     big[0:2, 0 : 2 * QUARTER] = outb[0:2, :]
     for block in reversed(range(1, PEERS)):
         there = opposite(block)
+        width = pl.ds(0, 2 * QUARTER if DIRECT[chunk_of(there)] else QUARTER)
         pltpu.make_async_remote_copy(
-            src_ref=outb.at[pl.ds(2 * block, 2), :],
-            dst_ref=big.at[pl.ds(2 * there, 2), pl.ds(0, 2 * QUARTER)],
+            src_ref=outb.at[pl.ds(2 * block, 2), width],
+            dst_ref=big.at[pl.ds(2 * there, 2), width],
             send_sem=d_send,
             recv_sem=d_recv.at[there // (NY * NC)],
             device_id=(ep_at(block), x),
@@ -302,9 +313,9 @@
 
     def arrived(ch):
         for p in (2 * ch + 1, 2 * ch):
-            messages(2 * GROUP - 4 * (p == 0), d_recv.at[p])
+            messages((GROUP // 2 - (p == 0)) * (4 if DIRECT[ch] else 2), d_recv.at[p])
         rows = pl.ds(ch * CHUNK, CHUNK)
-        for r in (1, 3):
+        for r in PARTNERS[DIRECT[ch]]:
             copy = along_tp(
                 r, big.at[rows, columns(0)], big.at[rows, columns(NX - r)],
                 ag_send.at[ch, r], ag_recv.at[ch, NX - r],
@@ -314,7 +325,7 @@
 
     def work(ch):
         rows = pl.ds(ch * CHUNK, CHUNK)
-        for r in (1, 3):
+        for r in PARTNERS[DIRECT[ch]]:
             block = big.at[rows, columns(r)]
             pltpu.make_async_copy(block, block, ag_recv.at[ch, r]).wait()
         pre = jnp.zeros((CHUNK, 256), F32)
@@ -329,9 +340,9 @@
         row_scale = jnp.sum(squares, axis=-1, keepdims=True) * (1.0 / D)
         row_scale = lax.rsqrt(row_scale + EPS)
         hidden = (silu(pre * row_scale) * (up * row_scale)).astype(BF)
-        for r in (1, 3, 2, 0):
+        for r in (2, 1, 3, 0):
             eparts[r, rows, :] = mm(hidden, ed[:, quarter(r)]).astype(BF)
-        for r in (1, 3):
+        for r in PARTNERS[DIRECT[ch]]:
             copy = along_tp(
                 r, eparts.at[r, rows, :], rs.at[NX - r, rows, :],
                 rs_send.at[ch, r], rs_recv.at[ch, NX - r],
@@ -353,7 +364,7 @@
     def give_back(ch):
         rows = pl.ds(ch * CHUNK, CHUNK)
         total = eparts[0, rows, :].astype(F32)
-        for r in (1, 3):
+        for r in PARTNERS[DIRECT[ch]]:
             block = rs.at[r, rows, :]
             pltpu.make_async_copy(block, block, rs_recv.at[ch, r]).wait()
             total = total + rs[r, rows, :].astype(F32)
@@ -363,6 +374,10 @@
             ret[0:2, :] = total[0:2]
         send_rows(rout, ret, b_send, b_recv, x, range(max(1, ch * CHUNK // 2), (ch + 1) * CHUNK // 2))
 
+    def straight(ch):
+        blocks = range(ch * CHUNK // 2, (ch + 1) * CHUNK // 2)
+        send_rows(eparts.at[2], ret2, o_send, o_recv, tps[2], blocks)
+
     arrived(3)
     arrived(2)
     arrived(1)
@@ -370,11 +385,10 @@
     l_eg.wait()
     l_eu.wait()
     l_ed.wait()
-    work(3)
-    work(2)
-    work(1)
-    work(0)
-    send_rows(eparts.at[2], ret2, o_send, o_recv, tps[2], range(PEERS))
+    for ch in reversed(range(CHUNKS)):
+        work(ch)
+        if DIRECT[ch]:
+            straight(ch)
     give_back(3)
     give_back(2)
     give_back(1)
@@ -393,7 +407,7 @@
     coarse = combine.astype(BF)
     fine = (combine - coarse.astype(F32)).astype(BF)
 
-    messages(2 * PEERS, o_recv)
+    messages(DIRECT.count(True) * CHUNK, o_recv)
     messages(2 * PEERS - 2, b_recv)
     back = (ret[...].astype(F32) + ret2[...].astype(F32)).astype(BF)
     over = (((0,), (0,)), ((), ()))
@@ -403,9 +417,9 @@
 
     for copy in shares:
         copy.wait_send()
-    messages(4 * PEERS - 4, d_send)
+    messages(sum(4 if DIRECT[chunk_of(opposite(b))] else 2 for b in range(1, PEERS)), d_send)
     messages(2 * PEERS - 2, b_send)
-    messages(2 * PEERS, o_send)
+    messages(DIRECT.count(True) * CHUNK, o_send)
 
 
 def shards(
@@ -413,7 +427,7 @@
     key_cache, value_cache, lengths, ffn_gain, routes, route_weight, expert_gate, expert_up,
     expert_down, dense_gate, dense_up, dense_down, gate_vector,
 ):
-    hbm = pl.BlockSpec(memory_space=pl.ANY)
+    hbm = pl.BlockSpec(memory_space=pltpu.HBM)
     vm = pltpu.VMEM
     dma = pltpu.SemaphoreType.DMA
     return pl.pallas_call(
@@ -443,9 +457,9 @@
             dma, dma, dma, dma, dma((NX,)), dma((NX,)), dma((NX,)), dma((NX,)),
         ],
         compiler_params=pltpu.CompilerParams(
-            collective_id=0, has_side_effects=True, vmem_limit_bytes=60 * 1024 * 1024
+            collective_id=0, has_side_effects=True, vmem_limit_bytes=50 * 1024 * 1024
         ),
-    )(
+    )(*[pltpu.with_memory_space_constraint(operand, pltpu.HBM) for operand in (
         lambdas, lengths,
         tokens, norm_gain.reshape(1, D), query_weight, key_weight, value_weight, output_weight,
         head_gain.reshape(1, 128), key_cache.reshape(SEQ, CACHE, 128),
@@ -453,7 +467,7 @@
         routes.T, route_weight.T,
         expert_gate.reshape(D, 256), expert_up.reshape(D, 256), expert_down.reshape(256, D),
         dense_gate, dense_up, dense_down, gate_vector.reshape(1, 512),
-    )
+    )])
 
 
 def solution(mesh):

time: 44.5 us -> 42.3 us (0.951)
  Pallas kernels: 43 us -> 41.6 us
  local copies, waits for them, and re-layouts: 1.32 us -> 0.61 us
    pallas_call x1, Pallas kernels: 43 us -> 41.6 us  [shards(): pl.pallas_call(kernel, name='layer', out_shape=jax.ShapeDtypeStruct((SEQ,...]
    unnamed x1, local copies, waits for them, and re-layouts: 1.32 us -> 0.61 us
where the time goes in v3:
time: 42.3 us
  Pallas kernels  41.6 us (98%)
  local copies, waits for them, and re-layouts  0.61 us (1%)
    pallas_call x1, Pallas kernels, shards(): pl.pallas_call(kernel, name='layer', out_shape=jax.ShapeDtypeStruct((SEQ,...  41.6 us

profile of v3, /device:TPU:1, one launch (start us, length us, event | category | flops | bytes accessed | tf_op | source)
XLA Modules:
  0.0 42.3 jit_solution(14736862106164456680)
XLA Ops:
  0.0 41.6 %layer.1 = bf16[16,512]{1,0:T(8,128)(2,1)S(1)} custom-call(f32[2]{0:T(128)} %lambdas_h.1, s32[16]{0:T(128)} %lengths_h.1, bf16[16,2048]{1,0:T(8,128)(2,1)} %tokens_h.1, f32[1,2048]{1,0:T(1,128)} %bitcast.16, bf16[2048,256]{1,0:T(8,128)(2,1)} %wq_h.1, bf16[2048,128]{1,0:T(8,128)(2,1)} %wk_h.1, bf16[2048,128]{1,0:T(8,128)(2,1)} %wv_h.1, ...), custom_call_target="tpu_custom_call" | custom-call | tf_op jit(solution)/shard_map/layer/pallas_call | solution.py:433
  41.6 0.6 %copy.23 = bf16[16,512]{1,0:T(8,128)(2,1)} copy(bf16[16,512]{1,0:T(8,128)(2,1)S(1)} %layer.1) | data formatting | bytes 32768

commit v4 on v3

--- a/solution.py
+++ b/solution.py
@@ -123,7 +123,8 @@
     for block in reversed(range(1, PEERS)):
         there = ep_at(block)
         pl.semaphore_signal(barrier, inc=1, device_id=(there, x), device_id_type=MESH)
-        pl.semaphore_signal(barrier, inc=1, device_id=(there, tps[2]), device_id_type=MESH)
+        if DIRECT[chunk_of(block)] or DIRECT[chunk_of(opposite(block))]:
+            pl.semaphore_signal(barrier, inc=1, device_id=(there, tps[2]), device_id_type=MESH)
 
     qs[...] = jnp.zeros((8 * SEQ, 128), F32)
     own[...] = jnp.zeros((8 * SEQ, 128), F32)
@@ -206,7 +207,8 @@
             share = mm(heads[:SEQ], wo[0:128, quarter(r)]) + mm(heads[SEQ:], wo[128:256, quarter(r)])
             ref[0, :, i * QUARTER : (i + 1) * QUARTER] = share.astype(BF)
 
-    pl.semaphore_wait(barrier, 2 * (PEERS - 1) + NX - 1)
+    straight_partners = sum(DIRECT[chunk_of(b)] or DIRECT[chunk_of(opposite(b))] for b in range(1, PEERS))
+    pl.semaphore_wait(barrier, PEERS - 1 + straight_partners + NX - 1)
 
     def along_tp(r, src, dst, send, recv):
         return pltpu.make_async_remote_copy(
@@ -223,9 +225,9 @@
         copy.start()
         shares.append(copy)
 
+    share_out(0, 2, near, near)
     share_out(0, 1, far, near)
     share_out(0, 3, far, near)
-    share_out(0, 2, near, near)
     share_out(1, 1, near, far)
     share_out(1, 3, near, far)
     share_out(1, 2, far, far)
@@ -385,10 +387,13 @@
     l_eg.wait()
     l_eu.wait()
     l_ed.wait()
-    for ch in reversed(range(CHUNKS)):
-        work(ch)
-        if DIRECT[ch]:
-            straight(ch)
+    work(3)
+    work(2)
+    work(1)
+    work(0)
+    straight(2)
+    straight(1)
+    straight(0)
     give_back(3)
     give_back(2)
     give_back(1)

time: 42.3 us -> 41.4 us (0.979)
  Pallas kernels: 41.6 us -> 40.7 us
    pallas_call x1, Pallas kernels: 41.6 us -> 40.7 us  [shards(): pl.pallas_call(kernel, name='layer', out_shape=jax.ShapeDtypeStruct((SEQ,...]
where the time goes in v4:
time: 41.4 us; the launch traced here: 41.3 us
  Pallas kernels  40.7 us (98%)
  local copies, waits for them, and re-layouts  0.61 us (1%)
    pallas_call x1, Pallas kernels, shards(): pl.pallas_call(kernel, name='layer', out_shape=jax.ShapeDtypeStruct((SEQ,...  40.7 us

profile of v4, /device:TPU:1, one launch (start us, length us, event | category | flops | bytes accessed | tf_op | source)
XLA Modules:
  0.0 41.3 jit_solution(13439281168082136018)
XLA Ops:
  0.0 40.7 %layer.1 = bf16[16,512]{1,0:T(8,128)(2,1)S(1)} custom-call(f32[2]{0:T(128)} %lambdas_h.1, s32[16]{0:T(128)} %lengths_h.1, bf16[16,2048]{1,0:T(8,128)(2,1)} %tokens_h.1, f32[1,2048]{1,0:T(1,128)} %bitcast.16, bf16[2048,256]{1,0:T(8,128)(2,1)} %wq_h.1, bf16[2048,128]{1,0:T(8,128)(2,1)} %wk_h.1, bf16[2048,128]{1,0:T(8,128)(2,1)} %wv_h.1, ...), custom_call_target="tpu_custom_call" | custom-call | tf_op jit(solution)/shard_map/layer/pallas_call | solution.py:438
  40.7 0.6 %copy.23 = bf16[16,512]{1,0:T(8,128)(2,1)} copy(bf16[16,512]{1,0:T(8,128)(2,1)S(1)} %layer.1) | data formatting | bytes 32768
